TPU v7x, 32 devices: a whole 2x2x4 slice. The times are simulated.
32 devices in a mesh: grp: 2 (over y), fs: 4 (over z), tp: 4 (over x, core).
Axes of the slice: x: 2, y: 2, z: 4, core: 2. Of those that a mesh axis runs over, the one named last changes fastest.
Arguments:
- tokens: bfloat16 [1024, 2048], P(('grp', 'fs')), parts along dimension 0, may hold values from -12 to 12, as said below
- mix_heads: bfloat16 [1024, 2048], P(('grp', 'fs'), 'tp'), parts along dimension 0, may hold values from -6 to 6
- norm_first: float32 [2048], replicated, may hold values from 0.1 to 1.9
- gate_first: bfloat16 [2048, 5632], P('fs', 'tp'), may hold values from -0.125 to 0.125
- up_first: bfloat16 [2048, 5632], P('fs', 'tp'), may hold values from -0.125 to 0.125
- down_first: bfloat16 [5632, 2048], P('tp', 'fs'), may hold values from -0.078125 to 0.078125
- out_weight: bfloat16 [2048, 2048], P('tp', 'fs'), may hold values from -0.125 to 0.125
- norm_second: float32 [2048], replicated, may hold values from 0.1 to 1.9
- gate_second: bfloat16 [2048, 5632], P('fs', 'tp'), may hold values from -0.125 to 0.125
- up_second: bfloat16 [2048, 5632], P('fs', 'tp'), may hold values from -0.125 to 0.125
- down_second: bfloat16 [5632, 2048], P('tp', 'fs'), may hold values from -0.078125 to 0.078125
Outputs:
- layer_out: bfloat16 [1024, 2048], P(('grp', 'fs')), parts along dimension 0
There are 2 independent parts, one for each index of `grp`. A program takes and returns all parts, laid end to end along the dimension named above; an argument that names none is the same for every part. Nothing has to cross between parts.
Inputs may be any that keep to these rules, and one draw needn't show every extreme that they name: Each row of tokens carries a scale of its own.
All inputs are finite; a program needn't handle non-finite values.
Results may differ from a plain program's by a relative error of at most 0.014.
Values may be sent and summed in bfloat16 or wider, within the bound.
A program may use at most 64 MiB of HBM per device.

v0:
```python
import jax
import jax.numpy as jnp
from jax import lax
from jax.sharding import PartitionSpec as P

EPS = 0.1


def norm_rows(row_block, gain_vector):
    widened = row_block.astype(jnp.float32)
    scaled = widened * lax.rsqrt(jnp.mean(widened * widened, axis=-1, keepdims=True) + EPS)
    return (scaled * gain_vector).astype(jnp.bfloat16)


def gate_values(normed, gate_weight, value_weight):
    whole_gate, whole_values = (
        lax.all_gather(gate_weight, "fs", axis=0, tiled=True),
        lax.all_gather(value_weight, "fs", axis=0, tiled=True),
    )
    return (
        jnp.dot(normed, whole_gate, preferred_element_type=jnp.float32),
        jnp.dot(normed, whole_values, preferred_element_type=jnp.float32),
    )


def half_branch(normed, gate_weight, value_weight, down_weight):
    gates, values = gate_values(normed, gate_weight, value_weight)
    hidden = (jax.nn.silu(gates) * values).astype(jnp.bfloat16)
    return 0.5 * jnp.dot(
        hidden,
        lax.all_gather(down_weight, "fs", axis=1, tiled=True),
        preferred_element_type=jnp.float32,
    )


def share_sum(block_terms):
    return lax.psum_scatter(
        block_terms.astype(jnp.bfloat16), "tp", scatter_dimension=0, tiled=True
    ).astype(jnp.float32)


def join_rows(row_block):
    return lax.all_gather(row_block, "tp", axis=0, tiled=True)


def local(
    tokens,
    mix_heads,
    norm_first,
    gate_first,
    up_first,
    down_first,
    out_weight,
    norm_second,
    gate_second,
    up_second,
    down_second,
):
    normed_one = norm_rows(tokens, norm_first)
    first_terms = half_branch(normed_one, gate_first, up_first, down_first)
    heads_out = jnp.dot(
        mix_heads,
        lax.all_gather(out_weight, "fs", axis=1, tiled=True),
        preferred_element_type=jnp.float32,
    )
    first_terms = first_terms + heads_out
    share_rows = tokens.shape[0] // lax.axis_size("tp")
    offset = lax.axis_index("tp") * share_rows
    own_rows = lax.dynamic_slice_in_dim(tokens, offset, share_rows, 0).astype(jnp.float32)
    resid_two = own_rows + share_sum(first_terms)
    normed_two = join_rows(norm_rows(resid_two, norm_second))
    second_terms = half_branch(normed_two, gate_second, up_second, down_second)
    finished = (resid_two + share_sum(second_terms)).astype(jnp.bfloat16)
    return join_rows(finished)


def solution(mesh):
    in_specs = (
        P(("grp", "fs"), None),
        P(("grp", "fs"), "tp"),
        P(),
        P("fs", "tp"),
        P("fs", "tp"),
        P("tp", "fs"),
        P("tp", "fs"),
        P(),
        P("fs", "tp"),
        P("fs", "tp"),
        P("tp", "fs"),
    )
    out_specs = P(("grp", "fs"), None)
    return jax.shard_map(local, mesh=mesh, in_specs=in_specs, out_specs=out_specs, check_vma=False)
```

profile of v0, /device:TPU:0, one launch (start us, length us, event | category | flops | bytes accessed | tf_op | source)
XLA Modules:
  0.0 763.6 jit_solution(13067139635178607233)
XLA Ops:
  6.5 0.7 all-gather.8.cloned.1.call-update
  7.3 0.7 all-gather.10.cloned.1.call-update
  8.0 0.0 all-gather.12.cloned.1.call-start
  8.1 0.7 all-gather.12.cloned.1.call-update
  8.8 0.5 all-gather.14.cloned.1.call-update
  9.3 0.0 reduce-scatter.3.cloned.1.call-start
  9.4 1.2 fusion.4
  10.6 107.7 %all-gather.8.cloned.1.call-done = bf16[2048,1408]{1,0:T(8,128)(2,1)} async-done(((bf16[512,1408]{1,0:T(8,128)(2,1)}), bf16[2048,1408]{1,0:T(8,128)(2,1)}) %all-gather.8.cloned.1.call-update) | async-done | bytes 5767184 | tf_op jit(solution)/shard_map/all_gather | solution.py:17
  118.3 3.9 fusion.11
  122.2 102.7 %all-gather.10.cloned.1.call-done = bf16[2048,1408]{1,0:T(8,128)(2,1)} async-done(((bf16[512,1408]{1,0:T(8,128)(2,1)}), bf16[2048,1408]{1,0:T(8,128)(2,1)}) %all-gather.10.cloned.1.call-update) | async-done | bytes 5767184 | tf_op jit(solution)/shard_map/all_gather | solution.py:18
  224.9 106.5 %all-gather.12.cloned.1.call-done = bf16[1408,2048]{1,0:T(8,128)(2,1)} async-done(((bf16[1408,512]{1,0:T(8,128)(2,1)}), bf16[1408,2048]{1,0:T(8,128)(2,1)}) %all-gather.12.cloned.1.call-update) | async-done | bytes 5767184 | tf_op jit(solution)/shard_map/all_gather | solution.py:31
  331.5 6.3 convolution_multiply_fusion.3
  337.8 39.1 %all-gather.14.cloned.1.call-done = bf16[512,2048]{1,0:T(8,128)(2,1)} async-done(((bf16[512,512]{1,0:T(8,128)(2,1)}), bf16[512,2048]{1,0:T(8,128)(2,1)}) %all-gather.14.cloned.1.call-update) | async-done | bytes 2097168 | tf_op jit(solution)/shard_map/all_gather | solution.py:63
  376.8 2.8 fusion
  379.7 0.0 all-gather.16.cloned.1.call-start
  379.8 0.5 all-gather.16.cloned.1.call-update
  380.3 0.7 all-gather.18.cloned.1.call-update
  381.1 0.7 all-gather.20.cloned.1.call-update
  381.8 0.0 reduce-scatter.5.cloned.1.call-start
  381.8 18.5 %reduce-scatter.3.cloned.1.call-done = bf16[32,2048]{1,0:T(8,128)(2,1)} async-done(((bf16[128,2048]{1,0:T(8,128)(2,1)}), bf16[32,2048]{1,0:T(8,128)(2,1)}) %reduce-scatter.3.cloned.1.call-update) | async-done | bytes 131088 | tf_op jit(solution)/shard_map/reduce_scatter | solution.py:37
  400.3 1.1 multiply_reduce_fusion
  401.4 1.0 multiply_convert_fusion
  402.4 6.6 all_gather.31
  409.0 99.5 %all-gather.16.cloned.1.call-done = bf16[2048,1408]{1,0:T(8,128)(2,1)} async-done(((bf16[512,1408]{1,0:T(8,128)(2,1)}), bf16[2048,1408]{1,0:T(8,128)(2,1)}) %all-gather.16.cloned.1.call-update) | async-done | bytes 5767184 | tf_op jit(solution)/shard_map/all_gather | solution.py:17
  508.5 3.6 fusion.15
  512.1 102.9 %all-gather.18.cloned.1.call-done = bf16[2048,1408]{1,0:T(8,128)(2,1)} async-done(((bf16[512,1408]{1,0:T(8,128)(2,1)}), bf16[2048,1408]{1,0:T(8,128)(2,1)}) %all-gather.18.cloned.1.call-update) | async-done | bytes 5767184 | tf_op jit(solution)/shard_map/all_gather | solution.py:18
  615.0 106.5 %all-gather.20.cloned.1.call-done = bf16[1408,2048]{1,0:T(8,128)(2,1)} async-done(((bf16[1408,512]{1,0:T(8,128)(2,1)}), bf16[1408,2048]{1,0:T(8,128)(2,1)}) %all-gather.20.cloned.1.call-update) | async-done | bytes 5767184 | tf_op jit(solution)/shard_map/all_gather | solution.py:31
  721.6 7.1 fusion.1
  728.6 20.0 %reduce-scatter.5.cloned.1.call-done = bf16[32,2048]{1,0:T(8,128)(2,1)} async-done(((bf16[128,2048]{1,0:T(8,128)(2,1)}), bf16[32,2048]{1,0:T(8,128)(2,1)}) %reduce-scatter.5.cloned.1.call-update) | async-done | bytes 131088 | tf_op jit(solution)/shard_map/reduce_scatter | solution.py:37
  748.7 1.0 add_convert_fusion
  749.7 6.6 all_gather.35
  756.3 0.8 copy.13
  (19 shorter events, 0.2 us)
Async XLA Ops:
  6.5 370.3 %copy-start = (bf16[128,512]{1,0:T(8,128)(2,1)S(1)}, bf16[128,512]{1,0:T(8,128)(2,1)}, u32[]{:S(2)}) copy-start(bf16[128,512]{1,0:T(8,128)(2,1)} %param.12) | copy-start | bytes 393220
  6.5 111.8 %all-gather.8.cloned.1.call-start = ((), (), s32[]{:S(2)}) async-start(), calls=%async_computation.2 | async-start | bytes 7208960 | tf_op jit(solution)/shard_map/all_gather | solution.py:17
  7.3 324.2 %copy-start.1 = (bf16[128,2048]{1,0:T(8,128)(2,1)S(1)}, bf16[128,2048]{1,0:T(8,128)(2,1)}, u32[]{:S(2)}) copy-start(bf16[128,2048]{1,0:T(8,128)(2,1)} %param.11) | copy-start | bytes 1572868
  7.3 324.2 %copy-start.3 = (f32[2048]{0:T(1024)S(1)}, f32[2048]{0:T(1024)}, u32[]{:S(2)}) copy-start(f32[2048]{0:T(1024)} %param.13) | copy-start | bytes 24580
  7.3 217.6 %all-gather.10.cloned.1.call-start = ((), (), s32[]{:S(2)}) async-start(), calls=%async_computation.3 | async-start | bytes 7208960 | tf_op jit(solution)/shard_map/all_gather | solution.py:18
  8.0 323.4 %all-gather.12.cloned.1.call-start = ((), (), s32[]{:S(2)}) async-start(), calls=%async_computation.4 | async-start | bytes 7208960 | tf_op jit(solution)/shard_map/all_gather | solution.py:31
  8.8 368.1 %all-gather.14.cloned.1.call-start = ((), (), s32[]{:S(2)}) async-start(), calls=%async_computation.5 | async-start | bytes 2621440 | tf_op jit(solution)/shard_map/all_gather | solution.py:63
  9.3 391.0 %reduce-scatter.3.cloned.1.call-start = ((), (), s32[]{:S(2)}) async-start(), calls=%async_computation.6 | async-start | bytes 655360 | tf_op jit(solution)/shard_map/reduce_scatter | solution.py:37
  337.8 63.6 %copy-start.4 = (f32[2048]{0:T(1024)S(1)}, f32[2048]{0:T(1024)}, u32[]{:S(2)}) copy-start(f32[2048]{0:T(1024)} %param.18) | copy-start | bytes 24580
  379.7 128.8 %all-gather.16.cloned.1.call-start = ((), (), s32[]{:S(2)}) async-start(), calls=%async_computation.7 | async-start | bytes 7208960 | tf_op jit(solution)/shard_map/all_gather | solution.py:17
  380.3 234.7 %all-gather.18.cloned.1.call-start = ((), (), s32[]{:S(2)}) async-start(), calls=%async_computation.8 | async-start | bytes 7208960 | tf_op jit(solution)/shard_map/all_gather | solution.py:18
  381.0 340.5 %all-gather.20.cloned.1.call-start = ((), (), s32[]{:S(2)}) async-start(), calls=%async_computation.9 | async-start | bytes 7208960 | tf_op jit(solution)/shard_map/all_gather | solution.py:31
  381.8 366.9 %reduce-scatter.5.cloned.1.call-start = ((), (), s32[]{:S(2)}) async-start(), calls=%async_computation.10 | async-start | bytes 655360 | tf_op jit(solution)/shard_map/reduce_scatter | solution.py:37
  512.1 236.6 %copy-start.2 = (bf16[32,2048]{1,0:T(8,128)(2,1)S(1)}, bf16[32,2048]{1,0:T(8,128)(2,1)}, u32[]{:S(2)}) copy-start(bf16[32,2048]{1,0:T(8,128)(2,1)} %reduce-scatter.3.cloned.1.call-done) | copy-start | bytes 393220
Sparse Core Ops, SparseCore 0:
  8.9 109.3 all-gather.7
  119.9 104.9 all-gather.9
  226.5 104.9 all-gather.11
  332.9 43.9 all-gather.13
  379.8 20.4 reduce-scatter.2
  401.7 106.6 all-gather.15
  510.0 104.9 all-gather.17
  616.6 104.9 all-gather.19
  728.8 19.8 reduce-scatter.4
where the time goes:
time: 764 us
  waiting for transfers between devices  708 us (93%)
  matrix products  23.7 us (3%)
  between operations  13.3 us (2%)
  blocking collectives  13.2 us (2%)
    all_gather x2, waiting for transfers between devices, half_branch(): lax.all_gather(down_weight, 'fs', axis=1, tiled=True)  213 us
    all_gather x2, waiting for transfers between devices, gate_values(): lax.all_gather(gate_weight, 'fs', axis=0, tiled=True)  207 us
    all_gather x2, waiting for transfers between devices, gate_values(): lax.all_gather(value_weight, 'fs', axis=0, tiled=True)  206 us
    all_gather x1, waiting for transfers between devices, local(): lax.all_gather(out_weight, 'fs', axis=1, tiled=True)  39.1 us
    reduce_scatter x2, waiting for transfers between devices, share_sum(): lax.psum_scatter(block_terms.astype(jnp.bfloat16), 'tp', scatter_dimensio...  38.5 us
  transfers between devices with their start and end apart: 9, of which 9 were waited for; matrix products, arithmetic and copies ran while one was open for 2% of the time, Pallas kernels for 0%

commit v1 on v0

--- a/solution.py
+++ b/solution.py
@@ -26,10 +26,33 @@
 def half_branch(normed, gate_weight, value_weight, down_weight):
     gates, values = gate_values(normed, gate_weight, value_weight)
     hidden = (jax.nn.silu(gates) * values).astype(jnp.bfloat16)
+
+    def fix_sums_all(my_data, axis_name, k_dim):
+        outer, built, shaped = (
+            lax.axis_size(axis_name),
+            lax.axis_index(axis_name),
+            my_data.shape[k_dim],
+        )
+        left_arr = lax.dynamic_update_slice_in_dim(
+            jnp.zeros(
+                [tick * outer if jj == k_dim else tick for jj, tick in enumerate(my_data.shape)],
+                my_data.dtype,
+            ),
+            my_data,
+            built * shaped,
+            axis=k_dim,
+        )
+        for w in tuple(range(1, outer)):
+            my_data = lax.ppermute(
+                my_data, axis_name, [(jj, (jj + 1) % outer) for jj in range(outer)]
+            )
+            left_arr = lax.dynamic_update_slice_in_dim(
+                left_arr, my_data, (built - w) % outer * shaped, axis=k_dim
+            )
+        return left_arr
+
     return 0.5 * jnp.dot(
-        hidden,
-        lax.all_gather(down_weight, "fs", axis=1, tiled=True),
-        preferred_element_type=jnp.float32,
+        hidden, fix_sums_all(down_weight, "fs", 1), preferred_element_type=jnp.float32
     )
 
 

time: 764 us -> 687 us (0.90)
  waiting for transfers between devices: 708 us -> 541 us
  starting transfers between devices: 0.31 us -> 65.3 us
  local copies, waits for them, and re-layouts: 0.82 us -> 22.8 us
    ppermute x0 -> x6, waiting for transfers between devices: none -> 314 us  [fix_sums_all(): lax.ppermute(my_data, axis_name, [(jj, (jj + 1) % outer) for jj in range(...]
    all_gather x2 -> x0, waiting for transfers between devices: 213 us -> none  [half_branch(): lax.all_gather(down_weight, 'fs', axis=1, tiled=True)]
    all_gather x2, waiting for transfers between devices: 207 us -> 15.1 us  [gate_values(): lax.all_gather(gate_weight, 'fs', axis=0, tiled=True)]
    ppermute x0 -> x6, starting transfers between devices: none -> 65.1 us  [fix_sums_all(): lax.ppermute(my_data, axis_name, [(jj, (jj + 1) % outer) for jj in range(...]
    all_gather x1, waiting for transfers between devices: 39.1 us -> 0.01 us  [local(): lax.all_gather(out_weight, 'fs', axis=1, tiled=True)]
    reduce_scatter x2, waiting for transfers between devices: 38.5 us -> 20 us  [share_sum(): lax.psum_scatter(block_terms.astype(jnp.bfloat16), 'tp', scatter_dimensio...]
    all_gather x2, waiting for transfers between devices: 206 us -> 189 us  [gate_values(): lax.all_gather(value_weight, 'fs', axis=0, tiled=True)]
    dynamic_update_slice x0 -> x8, local copies, waits for them, and re-layouts: none -> 15.5 us  [the longest x6 13.1 us: fix_sums_all(): lax.dynamic_update_slice_in_dim(left_arr, my_data, (built - w) % outer *...]
  transfers between devices with their start and end apart: 9 -> 13, of which waited for: 9 -> 10; matrix products, arithmetic and copies ran while one was open for 2% -> 5% of each run, Pallas kernels for 0% -> 0%
where the time goes in v1:
time: 687 us; the launch traced here: 686 us
  waiting for transfers between devices  541 us (79%)
  starting transfers between devices  65.3 us (10%)
  matrix products  25.6 us (4%)
  local copies, waits for them, and re-layouts  22.8 us (3%)
  blocking collectives  13.8 us (2%)
  between operations  13.6 us (2%)
    ppermute x6, waiting for transfers between devices, fix_sums_all(): lax.ppermute(my_data, axis_name, [(jj, (jj + 1) % outer) for jj in range(...  314 us
    all_gather x2, waiting for transfers between devices, gate_values(): lax.all_gather(value_weight, 'fs', axis=0, tiled=True)  189 us
    ppermute x6, starting transfers between devices, fix_sums_all(): lax.ppermute(my_data, axis_name, [(jj, (jj + 1) % outer) for jj in range(...  65.1 us
    reduce_scatter x2, waiting for transfers between devices, share_sum(): lax.psum_scatter(block_terms.astype(jnp.bfloat16), 'tp', scatter_dimensio...  20 us
    all_gather x2, waiting for transfers between devices, gate_values(): lax.all_gather(gate_weight, 'fs', axis=0, tiled=True)  15.1 us
    dot_general x2, matrix products, half_branch(): jnp.dot(hidden, fix_sums_all(down_weight, 'fs', 1), preferred_element_typ...  14.3 us
    all_gather x2, blocking collectives, join_rows(): return lax.all_gather(row_block, 'tp', axis=0, tiled=True)  13.8 us
  transfers between devices with their start and end apart: 13, of which 10 were waited for; matrix products, arithmetic and copies ran while one was open for 5% of the time, Pallas kernels for 0%

profile of v1, /device:TPU:0, one launch (start us, length us, event | category | flops | bytes accessed | tf_op | source)
XLA Modules:
  0.0 686.1 jit_solution(6384695306262801406)
XLA Ops:
  8.8 3.1 collective-permute-start
  11.9 56.6 %collective-permute-done = bf16[1408,512]{1,0:T(8,128)(2,1)} collective-permute-done((bf16[1408,512]{1,0:T(8,128)(2,1)}, bf16[1408,512]{1,0:T(8,128)(2,1)}, u32[]{:S(2)}, u32[]{:S(2)}) %collective-permute-start) | collective-permute-done | bytes 1441824 | tf_op jit(solution)/shard_map/ppermute | solution.py:46
  68.5 9.8 %collective-permute-start.1 = (bf16[1408,512]{1,0:T(8,128)(2,1)}, bf16[1408,512]{1,0:T(8,128)(2,1)S(1)}, u32[]{:S(2)}, u32[]{:S(2)}) collective-permute-start(bf16[1408,512]{1,0:T(8,128)(2,1)} %collective-permute-done), channel_id=1, source_target_pairs={{0,4},{4,8},{8,12},{12,0},{1,5},{5,9},{9,13},{13,1},{2,6},{6,10},{... | collective-permute-start | bytes 4325384 | tf_op jit(solution)/shard_map/ppermute | solution.py:46
  78.3 54.8 %collective-permute-done.1 = bf16[1408,512]{1,0:T(8,128)(2,1)S(1)} collective-permute-done((bf16[1408,512]{1,0:T(8,128)(2,1)}, bf16[1408,512]{1,0:T(8,128)(2,1)S(1)}, u32[]{:S(2)}, u32[]{:S(2)}) %collective-permute-start.1) | collective-permute-done | bytes 1441824 | tf_op jit(solution)/shard_map/ppermute | solution.py:46
  133.1 24.5 %collective-permute-start.2 = (bf16[1408,512]{1,0:T(8,128)(2,1)S(1)}, bf16[1408,512]{1,0:T(8,128)(2,1)}, u32[]{:S(2)}, u32[]{:S(2)}) collective-permute-start(bf16[1408,512]{1,0:T(8,128)(2,1)S(1)} %collective-permute-done.1), channel_id=1, source_target_pairs={{0,4},{4,8},{8,12},{12,0},{1,5},{5,9},{9,13},{13,1},{2,6},{6,10},{... | collective-permute-start | bytes 4325384 | tf_op jit(solution)/shard_map/ppermute | solution.py:46
  157.6 1.2 fusion.5
  158.9 3.2 broadcast.36.clone.1
  162.1 1.2 constant_dynamic-update-slice_fusion.7
  163.3 2.7 constant_dynamic-update-slice_fusion.6
  166.0 1.2 constant_dynamic-update-slice_fusion.5
  167.2 3.0 fusion.16
  170.3 48.3 %collective-permute-done.2 = bf16[1408,512]{1,0:T(8,128)(2,1)} collective-permute-done((bf16[1408,512]{1,0:T(8,128)(2,1)S(1)}, bf16[1408,512]{1,0:T(8,128)(2,1)}, u32[]{:S(2)}, u32[]{:S(2)}) %collective-permute-start.2) | collective-permute-done | bytes 1441824 | tf_op jit(solution)/shard_map/ppermute | solution.py:46
  218.5 2.7 constant_dynamic-update-slice_fusion.4
  221.2 15.1 %all-gather.6.cloned.1.call-done = bf16[2048,1408]{1,0:T(8,128)(2,1)} async-done(((bf16[512,1408]{1,0:T(8,128)(2,1)}), bf16[2048,1408]{1,0:T(8,128)(2,1)}) %all-gather.6.cloned.1.call-update) | async-done | bytes 5767184 | tf_op jit(solution)/shard_map/all_gather | solution.py:17
  236.3 4.5 fusion.12
  240.9 102.0 %all-gather.8.cloned.1.call-done = bf16[2048,1408]{1,0:T(8,128)(2,1)} async-done(((bf16[512,1408]{1,0:T(8,128)(2,1)}), bf16[2048,1408]{1,0:T(8,128)(2,1)}) %all-gather.8.cloned.1.call-update) | async-done | bytes 5767184 | tf_op jit(solution)/shard_map/all_gather | solution.py:18
  342.9 7.3 %fusion.1 = bf16[128,2048]{1,0:T(8,128)(2,1)} fusion(f32[128,2048]{1,0:T(8,128)S(1)} %copy-done.5, bf16[1408,2048]{1,0:T(8,128)(2,1)} %constant_dynamic-update-slice_fusion.4, bf16[2048,1408]{1,0:T(8,128)(2,1)} %all-gather.8.cloned.1.call-done, f32[128,1408]{1,0:T(8,128)} %fusion.12, bf16[128,2048]{1,0:T(8,128)(2,1)S(1)} %copy-done.1, ...), kind=kOutput, calls=%fused_computation.5 | convolution fusion | flops 1479311360 | bytes 14361088 | tf_op jit(solution)/shard_map/dot_general | solution.py:54
  351.5 38.1 %collective-permute-done.3 = bf16[1408,512]{1,0:T(8,128)(2,1)S(1)} collective-permute-done((bf16[1408,512]{1,0:T(8,128)(2,1)S(1)}, bf16[1408,512]{1,0:T(8,128)(2,1)S(1)}, u32[]{:S(2)}, u32[]{:S(2)}) %collective-permute-start.3) | collective-permute-done | bytes 1441824 | tf_op jit(solution)/shard_map/ppermute | solution.py:46
  389.6 65.9 %collective-permute-done.4 = bf16[1408,512]{1,0:T(8,128)(2,1)} collective-permute-done((bf16[1408,512]{1,0:T(8,128)(2,1)S(1)}, bf16[1408,512]{1,0:T(8,128)(2,1)}, u32[]{:S(2)}, u32[]{:S(2)}) %collective-permute-start.4) | collective-permute-done | bytes 1441824 | tf_op jit(solution)/shard_map/ppermute | solution.py:46
  455.5 27.6 %collective-permute-start.5 = (bf16[1408,512]{1,0:T(8,128)(2,1)}, bf16[1408,512]{1,0:T(8,128)(2,1)}, u32[]{:S(2)}, u32[]{:S(2)}) collective-permute-start(bf16[1408,512]{1,0:T(8,128)(2,1)} %collective-permute-done.4), channel_id=1, source_target_pairs={{0,4},{4,8},{8,12},{12,0},{1,5},{5,9},{9,13},{13,1},{2,6},{6,10},{... | collective-permute-start | bytes 4325384 | tf_op jit(solution)/shard_map/ppermute | solution.py:46
  483.1 3.2 broadcast.36.clone
  486.3 1.2 constant_dynamic-update-slice_fusion.3
  487.6 1.3 constant_dynamic-update-slice_fusion.2
  488.9 2.6 constant_dynamic-update-slice_fusion.1
  491.4 50.1 %collective-permute-done.5 = bf16[1408,512]{1,0:T(8,128)(2,1)} collective-permute-done((bf16[1408,512]{1,0:T(8,128)(2,1)}, bf16[1408,512]{1,0:T(8,128)(2,1)}, u32[]{:S(2)}, u32[]{:S(2)}) %collective-permute-start.5) | collective-permute-done | bytes 1441824 | tf_op jit(solution)/shard_map/ppermute | solution.py:46
  541.5 2.6 constant_dynamic-update-slice_fusion
  546.3 7.1 %all_gather.24 = bf16[128,2048]{1,0:T(8,128)(2,1)S(1)} all-gather(bf16[32,2048]{1,0:T(8,128)(2,1)S(1)} %multiply_convert_fusion), channel_id=1, replica_groups=mesh['grp'=2,'fs'=4,'tp'=4] {'tp'}, dimensions={0}, use_global_device_ids=true | all-gather | bytes 655360 | tf_op jit(solution)/shard_map/all_gather | solution.py:66
  553.4 3.7 fusion.17
  557.1 86.7 %all-gather.14.cloned.1.call-done = bf16[2048,1408]{1,0:T(8,128)(2,1)} async-done(((bf16[512,1408]{1,0:T(8,128)(2,1)}), bf16[2048,1408]{1,0:T(8,128)(2,1)}) %all-gather.14.cloned.1.call-update) | async-done | bytes 5767184 | tf_op jit(solution)/shard_map/all_gather | solution.py:18
  643.8 7.1 %fusion.2 = bf16[128,2048]{1,0:T(8,128)(2,1)} fusion(bf16[1408,2048]{1,0:T(8,128)(2,1)} %constant_dynamic-update-slice_fusion, bf16[128,2048]{1,0:T(8,128)(2,1)S(1)} %all_gather.24, bf16[2048,1408]{1,0:T(8,128)(2,1)} %all-gather.14.cloned.1.call-done, f32[128,1408]{1,0:T(8,128)S(1)} %fusion.17), kind=kOutput, calls=%fused_computation.6 | convolution fusion | flops 1478000640 | bytes 13303808 | tf_op jit(solution)/shard_map/dot_general | solution.py:54
  650.9 20.0 %reduce-scatter.5.cloned.1.call-done = bf16[32,2048]{1,0:T(8,128)(2,1)} async-done(((bf16[128,2048]{1,0:T(8,128)(2,1)}), bf16[32,2048]{1,0:T(8,128)(2,1)}) %reduce-scatter.5.cloned.1.call-update) | async-done | bytes 131088 | tf_op jit(solution)/shard_map/reduce_scatter | solution.py:60
  671.9 6.6 all_gather.27
  (41 shorter events, 7.4 us)
Async XLA Ops:
  6.5 160.7 %copy-start = (bf16[128,512]{1,0:T(8,128)(2,1)S(1)}, bf16[128,512]{1,0:T(8,128)(2,1)}, u32[]{:S(2)}) copy-start(bf16[128,512]{1,0:T(8,128)(2,1)} %param.12) | copy-start | bytes 393220
  6.5 155.5 %copy-start.2 = (bf16[1408,512]{1,0:T(8,128)(2,1)S(1)}, bf16[1408,512]{1,0:T(8,128)(2,1)}, u32[]{:S(2)}) copy-start(bf16[1408,512]{1,0:T(8,128)(2,1)} %param.16) | copy-start | bytes 4325380
  6.5 160.7 %all-gather.10.cloned.1.call-start = ((), (), s32[]{:S(2)}) async-start(), calls=%async_computation.4 | async-start | bytes 2621440 | tf_op jit(solution)/shard_map/all_gather | solution.py:86
  7.3 229.1 %all-gather.6.cloned.1.call-start = ((), (), s32[]{:S(2)}) async-start(), calls=%async_computation.2 | async-start | bytes 7208960 | tf_op jit(solution)/shard_map/all_gather | solution.py:17
  8.0 334.9 %all-gather.8.cloned.1.call-start = ((), (), s32[]{:S(2)}) async-start(), calls=%async_computation.3 | async-start | bytes 7208960 | tf_op jit(solution)/shard_map/all_gather | solution.py:18
  8.7 535.4 %reduce-scatter.3.cloned.1.call-start = ((), (), s32[]{:S(2)}) async-start(), calls=%async_computation.5 | async-start | bytes 655360 | tf_op jit(solution)/shard_map/reduce_scatter | solution.py:60
  8.8 59.8 %collective-permute-start = (bf16[1408,512]{1,0:T(8,128)(2,1)}, bf16[1408,512]{1,0:T(8,128)(2,1)}, u32[]{:S(2)}, u32[]{:S(2)}) collective-permute-start(bf16[1408,512]{1,0:T(8,128)(2,1)} %param.16), channel_id=1, source_target_pairs={{0,4},{4,8},{8,12},{12,0},{1,5},{5,9},{9,13},{13,1},{2,6},{6,10},{... | collective-permute-start | bytes 4325384 | tf_op jit(solution)/shard_map/ppermute | solution.py:46
  68.5 64.6 %collective-permute-start.1 = (bf16[1408,512]{1,0:T(8,128)(2,1)}, bf16[1408,512]{1,0:T(8,128)(2,1)S(1)}, u32[]{:S(2)}, u32[]{:S(2)}) collective-permute-start(bf16[1408,512]{1,0:T(8,128)(2,1)} %collective-permute-done), channel_id=1, source_target_pairs={{0,4},{4,8},{8,12},{12,0},{1,5},{5,9},{9,13},{13,1},{2,6},{6,10},{... | collective-permute-start | bytes 4325384 | tf_op jit(solution)/shard_map/ppermute | solution.py:46
  133.1 85.4 %collective-permute-start.2 = (bf16[1408,512]{1,0:T(8,128)(2,1)S(1)}, bf16[1408,512]{1,0:T(8,128)(2,1)}, u32[]{:S(2)}, u32[]{:S(2)}) collective-permute-start(bf16[1408,512]{1,0:T(8,128)(2,1)S(1)} %collective-permute-done.1), channel_id=1, source_target_pairs={{0,4},{4,8},{8,12},{12,0},{1,5},{5,9},{9,13},{13,1},{2,6},{6,10},{... | collective-permute-start | bytes 4325384 | tf_op jit(solution)/shard_map/ppermute | solution.py:46
  163.3 73.0 %copy-start.1 = (bf16[128,2048]{1,0:T(8,128)(2,1)S(1)}, bf16[128,2048]{1,0:T(8,128)(2,1)}, u32[]{:S(2)}) copy-start(bf16[128,2048]{1,0:T(8,128)(2,1)} %param.11) | copy-start | bytes 1572868
  163.3 73.0 %copy-start.6 = (f32[2048]{0:T(1024)S(1)}, f32[2048]{0:T(1024)}, u32[]{:S(2)}) copy-start(f32[2048]{0:T(1024)} %param.13) | copy-start | bytes 24580
  218.5 124.4 %copy-start.5 = (f32[128,2048]{1,0:T(8,128)S(1)}, f32[128,2048]{1,0:T(8,128)}, u32[]{:S(2)}) copy-start(f32[128,2048]{1,0:T(8,128)} %fusion.16) | copy-start | bytes 3145732
  240.9 110.6 %copy-start.3 = (bf16[1408,512]{1,0:T(8,128)(2,1)S(1)}, bf16[1408,512]{1,0:T(8,128)(2,1)}, u32[]{:S(2)}) copy-start(bf16[1408,512]{1,0:T(8,128)(2,1)} %param.21) | copy-start | bytes 4325380
  350.2 203.2 %all-gather.12.cloned.1.call-start = ((), (), s32[]{:S(2)}) async-start(), calls=%async_computation.6 | async-start | bytes 7208960 | tf_op jit(solution)/shard_map/all_gather | solution.py:17
  350.8 293.0 %all-gather.14.cloned.1.call-start = ((), (), s32[]{:S(2)}) async-start(), calls=%async_computation.7 | async-start | bytes 7208960 | tf_op jit(solution)/shard_map/all_gather | solution.py:18
  351.4 319.6 %reduce-scatter.5.cloned.1.call-start = ((), (), s32[]{:S(2)}) async-start(), calls=%async_computation.8 | async-start | bytes 655360 | tf_op jit(solution)/shard_map/reduce_scatter | solution.py:60
  351.4 38.1 %collective-permute-start.3 = (bf16[1408,512]{1,0:T(8,128)(2,1)S(1)}, bf16[1408,512]{1,0:T(8,128)(2,1)S(1)}, u32[]{:S(2)}, u32[]{:S(2)}) collective-permute-start(bf16[1408,512]{1,0:T(8,128)(2,1)S(1)} %copy-done.3), channel_id=1, source_target_pairs={{0,4},{4,8},{8,12},{12,0},{1,5},{5,9},{9,13},{13,1},{2,6},{6,10},{... | collective-permute-start | bytes 4325384 | tf_op jit(solution)/shard_map/ppermute | solution.py:46
  389.6 65.9 %collective-permute-start.4 = (bf16[1408,512]{1,0:T(8,128)(2,1)S(1)}, bf16[1408,512]{1,0:T(8,128)(2,1)}, u32[]{:S(2)}, u32[]{:S(2)}) collective-permute-start(bf16[1408,512]{1,0:T(8,128)(2,1)S(1)} %collective-permute-done.3), channel_id=1, source_target_pairs={{0,4},{4,8},{8,12},{12,0},{1,5},{5,9},{9,13},{13,1},{2,6},{6,10},{... | collective-permute-start | bytes 4325384 | tf_op jit(solution)/shard_map/ppermute | solution.py:46
  455.5 86.0 %collective-permute-start.5 = (bf16[1408,512]{1,0:T(8,128)(2,1)}, bf16[1408,512]{1,0:T(8,128)(2,1)}, u32[]{:S(2)}, u32[]{:S(2)}) collective-permute-start(bf16[1408,512]{1,0:T(8,128)(2,1)} %collective-permute-done.4), channel_id=1, source_target_pairs={{0,4},{4,8},{8,12},{12,0},{1,5},{5,9},{9,13},{13,1},{2,6},{6,10},{... | collective-permute-start | bytes 4325384 | tf_op jit(solution)/shard_map/ppermute | solution.py:46
  486.3 58.9 %copy-start.7 = (f32[2048]{0:T(1024)S(1)}, f32[2048]{0:T(1024)}, u32[]{:S(2)}) copy-start(f32[2048]{0:T(1024)} %param.18) | copy-start | bytes 24580
  557.1 113.8 %copy-start.4 = (bf16[32,2048]{1,0:T(8,128)(2,1)S(1)}, bf16[32,2048]{1,0:T(8,128)(2,1)}, u32[]{:S(2)}) copy-start(bf16[32,2048]{1,0:T(8,128)(2,1)} %reduce-scatter.3.cloned.1.call-done) | copy-start | bytes 393220
Sparse Core Ops, SparseCore 0:
  8.9 70.9 all-gather.9
  81.5 154.7 all-gather.5
  237.9 104.9 all-gather.7
  350.3 19.8 reduce-scatter.2
  371.7 165.0 all-gather.11
  538.2 105.5 all-gather.13
  651.0 19.8 reduce-scatter.4
